TPU v7x, 32 devices: a whole 2x2x4 slice. The times are simulated.
32 devices in a mesh: tp: 16 (over z, y, x), dp: 2 (over core).
Axes of the slice: x: 2, y: 2, z: 4, core: 2. Of those that a mesh axis runs over, the one named last changes fastest.
Arguments:
- hidden: bfloat16 [16, 4096], P(None, 'dp'), may hold values from -6 to 6
- norm_gain: float32 [2, 4096], P(None, 'dp'), may hold values from 0.1 to 1.9
- gate_weight: bfloat16 [2, 4096, 8192], P(None, 'dp', 'tp'), may hold values from -0.09375 to 0.09375
- inner_weight: bfloat16 [2, 4096, 8192], P(None, 'dp', 'tp'), may hold values from -0.09375 to 0.09375
- write_weight: bfloat16 [2, 4096, 2048], P(None, 'dp', 'tp'), may hold values from -0.09375 to 0.09375
- read_weight: bfloat16 [2, 4096, 2048], P(None, 'dp', 'tp'), may hold values from -0.09375 to 0.09375
- step_weight: bfloat16 [2, 4096, 128], P(None, 'dp'), may hold values from -0.09375 to 0.09375
- conv_inner: bfloat16 [2, 4, 8192], P(None, None, 'tp'), may hold values from -3 to 3
- conv_write: bfloat16 [2, 4, 2048], P(None, None, 'tp'), may hold values from -3 to 3
- conv_read: bfloat16 [2, 4, 2048], P(None, None, 'tp'), may hold values from -3 to 3
- step_bias: float32 [2, 128], P(None, 'tp'), may hold values from -4 to -1
- decay_log: float32 [2, 128], P(None, 'tp'), may hold values from -3 to 0.5
- skip_gain: float32 [2, 128], P(None, 'tp'), may hold values from 0.1 to 1.9
- group_gain: float32 [2, 8192], P(None, 'tp'), may hold values from 0.1 to 1.9
- out_weight: bfloat16 [2, 8192, 4096], P(None, 'tp', 'dp'), may hold values from -0.4 to 0.4
- state_inner: bfloat16 [2, 16, 3, 8192], P(None, 'dp', None, 'tp'), may hold values from -6 to 6
- state_write: bfloat16 [2, 16, 3, 2048], P(None, 'dp', None, 'tp'), may hold values from -6 to 6
- state_read: bfloat16 [2, 16, 3, 2048], P(None, 'dp', None, 'tp'), may hold values from -6 to 6
- recurrent: float32 [2, 16, 128, 64, 128], P(None, 'dp', 'tp'), may hold values from -1.2 to 1.2, as said below
Outputs:
- out_hidden: bfloat16 [16, 4096], P(None, 'dp')
- next_inner: bfloat16 [2, 16, 3, 8192], P(None, 'dp', None, 'tp')
- next_write: bfloat16 [2, 16, 3, 2048], P(None, 'dp', None, 'tp')
- next_read: bfloat16 [2, 16, 3, 2048], P(None, 'dp', None, 'tp')
- next_recurrent: float32 [2, 16, 128, 64, 128], P(None, 'dp', 'tp')
Inputs may be any that keep to these rules, and one draw needn't show every extreme that they name: recurrent states of order a tenth, with scales that differ between heads.
All inputs are finite; a program needn't handle non-finite values.
Results may differ from a plain program's by a relative error of at most 0.025.
Values may be sent and summed in bfloat16 or wider, within the bound.
A program may use at most 64 MiB of HBM per device.

v0:
```python
import jax
import jax.numpy as jnp
from jax import lax
from jax.sharding import PartitionSpec as P

D = 4096
HEADS = 128
GROUPS = 16
eps = 1e-06


def convolve(state, fresh_row, kernel):
    window = jnp.concatenate([state, fresh_row[:, None, :]], axis=1)
    summed = jnp.sum(window.astype(jnp.float32) * kernel.astype(jnp.float32)[None], axis=1)
    return (jax.nn.silu(summed), window[:, 1:])


def mixer_block(normed, number, weights):
    (
        gate_weight,
        inner_weight,
        write_weight,
        read_weight,
        step_weight,
        conv_inner,
        conv_write,
        conv_read,
        step_bias,
        decay_log,
        skip_gain,
        group_gain,
        out_weight,
        state_inner,
        state_write,
        state_read,
        recurrent,
    ) = weights

    def partial_of(weight):
        return jnp.dot(normed, weight[number], preferred_element_type=jnp.float32).astype(
            jnp.bfloat16
        )

    summed = (
        lax.psum_scatter(partial_of(gate_weight), "dp", scatter_dimension=0, tiled=True).astype(
            jnp.float32
        ),
        lax.psum_scatter(partial_of(inner_weight), "dp", scatter_dimension=0, tiled=True).astype(
            jnp.float32
        ),
        lax.psum_scatter(partial_of(write_weight), "dp", scatter_dimension=0, tiled=True).astype(
            jnp.float32
        ),
        lax.psum_scatter(partial_of(read_weight), "dp", scatter_dimension=0, tiled=True).astype(
            jnp.float32
        ),
        lax.psum_scatter(partial_of(step_weight), "dp", scatter_dimension=0, tiled=True).astype(
            jnp.float32
        ),
    )
    gate_raw, inner_raw, write_raw, read_raw, step_raw = [
        member.astype(jnp.bfloat16) for member in summed
    ]
    inner_act, next_inner = convolve(state_inner[number], inner_raw, conv_inner[number])
    write_act, next_write = convolve(state_write[number], write_raw, conv_write[number])
    read_act, next_read = convolve(state_read[number], read_raw, conv_read[number])
    write_all, read_all = (
        lax.all_gather(write_act.astype(jnp.bfloat16), "tp", axis=1, tiled=True),
        lax.all_gather(read_act.astype(jnp.bfloat16), "tp", axis=1, tiled=True),
    )
    heads_here = step_bias.shape[1]
    head_dim = recurrent.shape[3]
    state_dim = recurrent.shape[4]
    rows_here = inner_act.shape[0]
    first_head = lax.axis_index("tp") * heads_here
    group_index = first_head // (HEADS // GROUPS)
    write_grid = write_all.reshape(rows_here, state_dim, GROUPS)
    read_grid = read_all.reshape(rows_here, state_dim, GROUPS)
    write_vec = lax.dynamic_slice_in_dim(write_grid, group_index, 1, 2)[:, :, 0].astype(jnp.float32)
    read_vec = lax.dynamic_slice_in_dim(read_grid, group_index, 1, 2)[:, :, 0].astype(jnp.float32)
    step_own = lax.dynamic_slice_in_dim(step_raw, first_head, heads_here, 1)
    step_size = jax.nn.softplus(step_own.astype(jnp.float32) + step_bias[number][None, :])
    retain = jnp.exp(-step_size * jnp.exp(decay_log[number])[None, :])
    inner_heads = inner_act.reshape(rows_here, heads_here, head_dim)
    updated = (
        retain[:, :, None, None] * recurrent[number]
        + (step_size[:, :, None] * inner_heads)[:, :, :, None] * write_vec[:, None, None, :]
    )
    readout = jnp.einsum("bhpn,bn->bhp", updated, read_vec, precision=lax.Precision.HIGHEST)
    readout = readout + skip_gain[number][None, :, None] * inner_heads
    gated_out = readout.reshape(rows_here, heads_here * head_dim) * jax.nn.silu(
        gate_raw.astype(jnp.float32)
    )
    selector = (jnp.arange(GROUPS) == group_index).astype(jnp.float32)
    totals = lax.psum(jnp.sum(gated_out * gated_out, axis=1)[:, None] * selector[None, :], "tp")
    group_sum = jnp.sum(totals * selector[None, :], axis=1, keepdims=True)
    group_factor = lax.rsqrt(group_sum / (HEADS // GROUPS * head_dim) + eps)
    group_normed = (gated_out * group_factor * group_gain[number][None, :]).astype(jnp.bfloat16)
    branch = jnp.dot(
        lax.all_gather(group_normed, "dp", axis=0, tiled=True),
        out_weight[number],
        preferred_element_type=jnp.float32,
    )
    return (branch, (next_inner, next_write, next_read, updated))


def total_over(branch):
    return lax.psum(branch, "tp")


def local(
    hidden,
    norm_gain,
    gate_weight,
    inner_weight,
    write_weight,
    read_weight,
    step_weight,
    conv_inner,
    conv_write,
    conv_read,
    step_bias,
    decay_log,
    skip_gain,
    group_gain,
    out_weight,
    state_inner,
    state_write,
    state_read,
    recurrent,
):
    weights = (
        gate_weight,
        inner_weight,
        write_weight,
        read_weight,
        step_weight,
        conv_inner,
        conv_write,
        conv_read,
        step_bias,
        decay_log,
        skip_gain,
        group_gain,
        out_weight,
        state_inner,
        state_write,
        state_read,
        recurrent,
    )
    wide_in = hidden.astype(jnp.float32)
    squares = lax.psum(jnp.sum(wide_in * wide_in, axis=1, keepdims=True), "dp")
    normed = (wide_in * lax.rsqrt(squares / D + eps) * norm_gain[0][None, :]).astype(jnp.bfloat16)
    branch, first_states = mixer_block(normed, 0, weights)
    middle = (wide_in + total_over(branch)).astype(jnp.bfloat16).astype(jnp.float32)
    squares = lax.psum(jnp.sum(middle * middle, axis=1, keepdims=True), "dp")
    normed = (middle * lax.rsqrt(squares / D + eps) * norm_gain[1][None, :]).astype(jnp.bfloat16)
    branch, second_states = mixer_block(normed, 1, weights)
    result = (middle + total_over(branch)).astype(jnp.bfloat16)
    stacked = [jnp.stack([earlier, later]) for earlier, later in zip(first_states, second_states)]
    return (result, stacked[0], stacked[1], stacked[2], stacked[3])


def solution(mesh):
    return jax.shard_map(
        local,
        mesh=mesh,
        in_specs=(
            P(None, "dp"),
            P(None, "dp"),
            P(None, "dp", "tp"),
            P(None, "dp", "tp"),
            P(None, "dp", "tp"),
            P(None, "dp", "tp"),
            P(None, "dp", None),
            P(None, None, "tp"),
            P(None, None, "tp"),
            P(None, None, "tp"),
            P(None, "tp"),
            P(None, "tp"),
            P(None, "tp"),
            P(None, "tp"),
            P(None, "tp", "dp"),
            P(None, "dp", None, "tp"),
            P(None, "dp", None, "tp"),
            P(None, "dp", None, "tp"),
            P(None, "dp", "tp", None, None),
        ),
        out_specs=(
            P(None, "dp"),
            P(None, "dp", None, "tp"),
            P(None, "dp", None, "tp"),
            P(None, "dp", None, "tp"),
            P(None, "dp", "tp", None, None),
        ),
        check_vma=False,
    )
```

profile of v0, /device:TPU:0, one launch (start us, length us, event | category | flops | bytes accessed | tf_op | source)
XLA Modules:
  0.0 509.0 jit_solution(9227752754220769065)
XLA Ops:
  7.2 1.0 fusion.58
  8.2 2.6 psum.42
  10.8 0.8 fusion.97
  11.8 2.8 fusion.28
  14.7 2.6 fusion.31
  17.4 0.6 dynamic-slice
  18.8 0.2 convolution_convert_fusion.4
  19.1 0.2 convolution_convert_fusion.3
  19.3 1.3 convolution_convert_fusion.5
  20.6 3.5 all-reduce.7
  24.2 42.2 %all_gather.18 = bf16[8,2048]{1,0:T(8,128)(2,1)S(1)} all-gather(bf16[8,128]{1,0:T(8,128)(2,1)S(1)} %multiply_convert_fusion.5), channel_id=1, replica_groups=mesh['tp'=16,'dp'=2] {'tp'}, dimensions={1}, use_global_device_ids=true | all-gather | bytes 34816 | tf_op jit(solution)/shard_map/all_gather | solution.py:68
  66.4 35.6 %all_gather.19 = bf16[8,2048]{1,0:T(8,128)(2,1)S(1)} all-gather(bf16[8,128]{1,0:T(8,128)(2,1)S(1)} %multiply_convert_fusion.4), channel_id=1, replica_groups=mesh['tp'=16,'dp'=2] {'tp'}, dimensions={1}, use_global_device_ids=true | all-gather | bytes 34816 | tf_op jit(solution)/shard_map/all_gather | solution.py:69
  102.0 0.2 reshape.108
  102.2 0.3 dynamic-slice_reduce_fusion.1
  102.5 0.2 reshape.107
  102.7 0.2 convert_reduce_fusion.1
  103.0 0.1 multiply_exponential_fusion.1
  103.2 0.7 multiply_reduce_fusion.1
  103.9 0.1 reduce_sum.114
  103.9 0.1 broadcast_multiply_fusion.1
  104.0 4.2 fusion.16
  108.3 0.1 multiply_add_fusion.3
  108.3 0.1 reshape.109
  108.4 0.8 multiply_reduce_fusion.5
  109.3 38.6 %psum.43 = f32[8,16]{1,0:T(8,128)S(1)} all-reduce(f32[8,16]{1,0:T(8,128)S(1)} %broadcast_multiply_fusion.3), channel_id=1, replica_groups=mesh['tp'=16,'dp'=2] {'tp'}, use_global_device_ids=true, to_apply=%region_11.12 | all-reduce | flops 128 | bytes 1024 | tf_op jit(solution)/shard_map/psum | solution.py:95
  147.9 0.1 multiply_reduce_fusion.9
  148.0 0.8 multiply_convert_fusion.1
  148.8 1.8 all_gather.20
  150.6 2.6 fusion.9
  153.4 101.5 %all-reduce.11.cloned.1.call-done = f32[16,2048]{1,0:T(8,128)} async-done(((f32[16,2048]{1,0:T(8,128)}), f32[16,2048]{1,0:T(8,128)}) %all-reduce.11.cloned.1.call-update) | async-done | bytes 131088 | tf_op jit(solution)/shard_map/psum | solution.py:108
  254.8 1.0 fusion.62
  255.9 2.5 psum.45
  258.4 0.2 convolution_convert_fusion.1
  258.6 0.2 convolution_convert_fusion
  258.8 1.3 convolution_convert_fusion.2
  260.1 2.6 fusion.34
  262.8 2.6 fusion.37
  265.4 3.3 all-reduce.6
  268.8 0.6 pad_maximum_fusion.4
  269.5 0.6 pad_maximum_fusion.5
  270.1 38.9 %all_gather.21 = bf16[8,2048]{1,0:T(8,128)(2,1)S(1)} all-gather(bf16[8,128]{1,0:T(8,128)(2,1)S(1)} %multiply_convert_fusion.3), channel_id=1, replica_groups=mesh['tp'=16,'dp'=2] {'tp'}, dimensions={1}, use_global_device_ids=true | all-gather | bytes 34816 | tf_op jit(solution)/shard_map/all_gather | solution.py:68
  308.9 0.2 reshape.110
  309.1 35.6 %all_gather.22 = bf16[8,2048]{1,0:T(8,128)(2,1)S(1)} all-gather(bf16[8,128]{1,0:T(8,128)(2,1)S(1)} %multiply_convert_fusion.2), channel_id=1, replica_groups=mesh['tp'=16,'dp'=2] {'tp'}, dimensions={1}, use_global_device_ids=true | all-gather | bytes 34816 | tf_op jit(solution)/shard_map/all_gather | solution.py:69
  344.8 0.2 reshape.111
  345.0 0.3 dynamic-slice_reduce_fusion
  345.3 0.3 convert_reduce_fusion
  345.6 0.1 multiply_exponential_fusion
  345.7 0.7 multiply_reduce_fusion
  346.4 0.1 reduce_sum.121
  346.5 0.1 broadcast_multiply_fusion
  346.6 4.2 multiply_add_fusion.1
  350.8 2.8 fusion.7
  353.6 0.1 multiply_add_fusion.2
  353.7 0.1 reshape.112
  353.8 0.8 multiply_reduce_fusion.2
  354.7 39.1 %psum.46 = f32[8,16]{1,0:T(8,128)S(1)} all-reduce(f32[8,16]{1,0:T(8,128)S(1)} %broadcast_multiply_fusion.2), channel_id=1, replica_groups=mesh['tp'=16,'dp'=2] {'tp'}, use_global_device_ids=true, to_apply=%region_25.26 | all-reduce | flops 128 | bytes 1024 | tf_op jit(solution)/shard_map/psum | solution.py:95
  393.8 0.1 multiply_reduce_fusion.8
  393.9 0.8 multiply_convert_fusion
  394.7 1.8 all_gather.23
  396.5 2.6 fusion
  399.1 4.1 pad_maximum_fusion
  403.2 0.6 pad_maximum_fusion.1
  403.8 96.8 %all-reduce.13.cloned.1.call-done = f32[16,2048]{1,0:T(8,128)} async-done(((f32[16,2048]{1,0:T(8,128)}), f32[16,2048]{1,0:T(8,128)}) %all-reduce.13.cloned.1.call-update) | async-done | bytes 131088 | tf_op jit(solution)/shard_map/psum | solution.py:108
  500.6 1.6 fusion.65
  (85 shorter events, 0.8 us)
Async XLA Ops:
  7.2 7.5 %copy-start.1 = (bf16[16,2048]{1,0:T(8,128)(2,1)S(1)}, bf16[16,2048]{1,0:T(8,128)(2,1)}, u32[]{:S(2)}) copy-start(bf16[16,2048]{1,0:T(8,128)(2,1)} %param.19) | copy-start | bytes 196612
  7.2 96.0 %reduce-scatter.5.cloned.1.call-start = ((), (), s32[]{:S(2)}) async-start(), calls=%async_computation.4 | async-start | bytes 24576 | tf_op jit(solution)/shard_map/reduce_scatter | solution.py:48
  11.7 5.8 %copy-start.16 = (u32[32]{0:T(128)S(1)}, u32[32]{0:T(128)}, u32[]{:S(2)}) copy-start(u32[32]{0:T(128)} %constant.63) | copy-start | bytes 388
  11.7 7.0 %copy-start.11 = (f32[2,8]{1,0:T(2,128)S(1)}, f32[2,8]{1,0:T(2,128)}, u32[]{:S(2)}) copy-start(f32[2,8]{1,0:T(2,128)} %param.31) | copy-start | bytes 196
  11.7 7.0 %copy-start.9 = (bf16[2,4,128]{2,1,0:T(4,128)(2,1)S(1)}, bf16[2,4,128]{2,1,0:T(4,128)(2,1)}, u32[]{:S(2)}) copy-start(bf16[2,4,128]{2,1,0:T(4,128)(2,1)} %param.27) | copy-start | bytes 6148
  11.7 7.0 %copy-start.10 = (bf16[2,4,128]{2,1,0:T(4,128)(2,1)S(1)}, bf16[2,4,128]{2,1,0:T(4,128)(2,1)}, u32[]{:S(2)}) copy-start(bf16[2,4,128]{2,1,0:T(4,128)(2,1)} %param.28) | copy-start | bytes 6148
  11.7 7.0 %copy-start.8 = (f32[2,512]{1,0:T(2,128)S(1)}, f32[2,512]{1,0:T(2,128)}, u32[]{:S(2)}) copy-start(f32[2,512]{1,0:T(2,128)} %param.32) | copy-start | bytes 12292
  11.7 7.1 %copy-start.5 = (bf16[2,8,3,128]{3,1,2,0:T(8,128)(2,1)S(1)}, bf16[2,8,3,128]{3,1,2,0:T(8,128)(2,1)}, u32[]{:S(2)}) copy-start(bf16[2,8,3,128]{3,1,2,0:T(8,128)(2,1)} %param.35) | copy-start | bytes 36868
  11.7 7.1 %copy-start.6 = (bf16[2,8,3,128]{3,1,2,0:T(8,128)(2,1)S(1)}, bf16[2,8,3,128]{3,1,2,0:T(8,128)(2,1)}, u32[]{:S(2)}) copy-start(bf16[2,8,3,128]{3,1,2,0:T(8,128)(2,1)} %param.36) | copy-start | bytes 36868
  11.7 7.1 %copy-start.14 = (bf16[2,2048,128]{2,1,0:T(8,128)(2,1)S(1)}, bf16[2,2048,128]{2,1,0:T(8,128)(2,1)}, u32[]{:S(2)}) copy-start(bf16[2,2048,128]{2,1,0:T(8,128)(2,1)} %param.23) | copy-start | bytes 3145732
  11.8 7.3 %copy-start.15 = (bf16[2,2048,128]{2,1,0:T(8,128)(2,1)S(1)}, bf16[2,2048,128]{2,1,0:T(8,128)(2,1)}, u32[]{:S(2)}) copy-start(bf16[2,2048,128]{2,1,0:T(8,128)(2,1)} %param.24) | copy-start | bytes 3145732
  14.6 9.5 %copy-start.7 = (bf16[2,4,512]{2,1,0:T(4,128)(2,1)S(1)}, bf16[2,4,512]{2,1,0:T(4,128)(2,1)}, u32[]{:S(2)}) copy-start(bf16[2,4,512]{2,1,0:T(4,128)(2,1)} %param.26) | copy-start | bytes 24580
  14.6 87.4 %copy-start.2 = (bf16[2,8,3,512]{3,1,2,0:T(8,128)(2,1)S(1)}, bf16[2,8,3,512]{3,1,2,0:T(8,128)(2,1)}, u32[]{:S(2)}) copy-start(bf16[2,8,3,512]{3,1,2,0:T(8,128)(2,1)} %param.34) | copy-start | bytes 147460
  14.6 93.8 %reduce-scatter.7.cloned.1.call-start = ((), (), s32[]{:S(2)}) async-start(), calls=%async_computation.5 | async-start | bytes 24576 | tf_op jit(solution)/shard_map/reduce_scatter | solution.py:45
  17.3 85.7 %copy-start.12 = (f32[2,8]{1,0:T(2,128)S(1)}, f32[2,8]{1,0:T(2,128)}, u32[]{:S(2)}) copy-start(f32[2,8]{1,0:T(2,128)} %param.30) | copy-start | bytes 196
  17.3 85.7 %copy-start.13 = (f32[2,8]{1,0:T(2,128)S(1)}, f32[2,8]{1,0:T(2,128)}, u32[]{:S(2)}) copy-start(f32[2,8]{1,0:T(2,128)} %param.29) | copy-start | bytes 196
  17.3 237.5 %all-reduce.11.cloned.1.call-start = ((), (), s32[]{:S(2)}) async-start(), calls=%async_computation.6 | async-start | bytes 262144 | tf_op jit(solution)/shard_map/psum | solution.py:108
  104.0 49.3 %copy-start.3 = (bf16[8,512]{1,0:T(8,128)(2,1)S(1)}, bf16[8,512]{1,0:T(8,128)(2,1)}, u32[]{:S(2)}) copy-start(bf16[8,512]{1,0:T(8,128)(2,1)} %reduce-scatter.5.cloned.1.call-done) | copy-start | bytes 24580
  153.3 192.4 %reduce-scatter.9.cloned.1.call-start = ((), (), s32[]{:S(2)}) async-start(), calls=%async_computation.7 | async-start | bytes 24576 | tf_op jit(solution)/shard_map/reduce_scatter | solution.py:48
  268.8 85.0 %reduce-scatter.11.cloned.1.call-start = ((), (), s32[]{:S(2)}) async-start(), calls=%async_computation.8 | async-start | bytes 24576 | tf_op jit(solution)/shard_map/reduce_scatter | solution.py:45
  345.5 155.1 %all-reduce.13.cloned.1.call-start = ((), (), s32[]{:S(2)}) async-start(), calls=%async_computation.9 | async-start | bytes 262144 | tf_op jit(solution)/shard_map/psum | solution.py:108
  346.6 4.2 copy-start
  399.1 4.1 copy-start.4
Sparse Core Ops, SparseCore 0:
  14.7 10.0 reduce-scatter.4
  27.6 8.6 reduce-scatter.6
  153.4 101.3 all-reduce.10
  268.9 6.5 reduce-scatter.8
  345.7 5.2 reduce-scatter.10
  399.3 101.3 all-reduce.12
where the time goes:
time: 510 us; the launch traced here: 509 us
  blocking collectives  245 us (48%)
  waiting for transfers between devices  198 us (39%)
  matrix products  26.6 us (5%)
  other arithmetic  19.8 us (4%)
  between operations  15.3 us (3%)
    psum x2, waiting for transfers between devices, total_over(): return lax.psum(branch, 'tp')  198 us
    all_gather x2, blocking collectives, mixer_block(): lax.all_gather(write_act.astype(jnp.bfloat16), 'tp', axis=1, tiled=True)  81.1 us
    psum x2, blocking collectives, mixer_block(): lax.psum(jnp.sum(gated_out * gated_out, axis=1)[:, None] * selector[None,...  77.7 us
    all_gather x2, blocking collectives, mixer_block(): lax.all_gather(read_act.astype(jnp.bfloat16), 'tp', axis=1, tiled=True)  71.2 us
    dot_general x10, matrix products, partial_of(): jnp.dot(normed, weight[number], preferred_element_type=jnp.float32)  14.2 us
  transfers between devices with their start and end apart: 6, of which 2 were waited for; matrix products, arithmetic and copies ran while one was open for 5% of the time, Pallas kernels for 0%

commit v1 on v0

--- a/solution.py
+++ b/solution.py
@@ -66,7 +66,12 @@
     read_act, next_read = convolve(state_read[number], read_raw, conv_read[number])
     write_all, read_all = (
         lax.all_gather(write_act.astype(jnp.bfloat16), "tp", axis=1, tiled=True),
-        lax.all_gather(read_act.astype(jnp.bfloat16), "tp", axis=1, tiled=True),
+        jnp.concatenate(
+            lax.all_to_all(
+                jnp.stack([read_act.astype(jnp.bfloat16)] * lax.axis_size("tp")), "tp", 0, 0
+            ),
+            axis=1,
+        ),
     )
     heads_here = step_bias.shape[1]
     head_dim = recurrent.shape[3]

time: 510 us -> 456 us (0.89)
  blocking collectives: 245 us -> 171 us
  starting transfers between devices: 0.25 us -> 12.9 us
  waiting for transfers between devices: 198 us -> 206 us
    all_gather x2 -> x0, blocking collectives: 71.2 us -> none  [mixer_block(): lax.all_gather(read_act.astype(jnp.bfloat16), 'tp', axis=1, tiled=True)]
    all_to_all x0 -> x2, starting transfers between devices: none -> 12.7 us  [mixer_block(): lax.all_to_all(jnp.stack([read_act.astype(jnp.bfloat16)] * lax.axis_size(...]
    psum x2, waiting for transfers between devices: 198 us -> 206 us  [total_over(): return lax.psum(branch, 'tp')]
  transfers between devices with their start and end apart: 6 -> 8, of which waited for: 2 -> 2; matrix products, arithmetic and copies ran while one was open for 5% -> 6% of each run, Pallas kernels for 0% -> 0%
where the time goes in v1:
time: 456 us; the launch traced here: 455 us
  waiting for transfers between devices  206 us (45%)
  blocking collectives  171 us (38%)
  matrix products  27.8 us (6%)
  other arithmetic  17.7 us (4%)
  between operations  15.4 us (3%)
  starting transfers between devices  12.9 us (3%)
    psum x2, waiting for transfers between devices, total_over(): return lax.psum(branch, 'tp')  206 us
    all_gather x2, blocking collectives, mixer_block(): lax.all_gather(write_act.astype(jnp.bfloat16), 'tp', axis=1, tiled=True)  82.2 us
    psum x2, blocking collectives, mixer_block(): lax.psum(jnp.sum(gated_out * gated_out, axis=1)[:, None] * selector[None,...  73.1 us
    dot_general x10, matrix products, partial_of(): jnp.dot(normed, weight[number], preferred_element_type=jnp.float32)  14.1 us
    all_to_all x2, starting transfers between devices, mixer_block(): lax.all_to_all(jnp.stack([read_act.astype(jnp.bfloat16)] * lax.axis_size(...  12.7 us
  transfers between devices with their start and end apart: 8, of which 2 were waited for; matrix products, arithmetic and copies ran while one was open for 6% of the time, Pallas kernels for 0%

profile of v1, /device:TPU:0, one launch (start us, length us, event | category | flops | bytes accessed | tf_op | source)
XLA Modules:
  0.0 455.3 jit_solution(13492545874779061188)
XLA Ops:
  7.3 1.1 fusion.58
  8.4 2.6 psum.42
  11.0 0.8 fusion.97
  11.8 2.7 fusion.28
  14.7 0.2 convolution_convert_fusion.4
  14.9 0.2 convolution_convert_fusion.3
  15.2 1.3 convolution_convert_fusion.5
  16.5 0.6 dynamic-slice
  17.7 3.5 all-reduce.7
  21.2 0.6 stack.24
  21.8 8.0 %all-to-all-start = ((bf16[16,8,128]{2,1,0:T(8,128)(2,1)}), bf16[16,8,128]{2,1,0:T(8,128)(2,1)S(1)}, u32[]{:S(2)}, u32[]{:S(2)}) async-start(bf16[16,8,128]{2,1,0:T(8,128)(2,1)} %stack.24), calls=%async_computation.1 | async-start | bytes 65536 | tf_op jit(solution)/shard_map/all_to_all | solution.py:70
  29.9 2.6 fusion.31
  32.8 41.1 %all_gather.12 = bf16[8,2048]{1,0:T(8,128)(2,1)S(1)} all-gather(bf16[8,128]{1,0:T(8,128)(2,1)S(1)} %multiply_convert_fusion.5), channel_id=1, replica_groups=mesh['tp'=16,'dp'=2] {'tp'}, dimensions={1}, use_global_device_ids=true | all-gather | bytes 34816 | tf_op jit(solution)/shard_map/all_gather | solution.py:68
  73.9 0.2 reshape.111
  74.2 0.2 convert_reduce_fusion.1
  74.5 0.1 multiply_exponential_fusion.1
  74.6 0.7 multiply_reduce_fusion.1
  75.3 0.1 reduce_sum.114
  75.4 0.1 broadcast_multiply_fusion.1
  75.5 0.2 reshape_reshape.6
  75.7 0.3 dynamic-slice_reduce_fusion.1
  76.0 4.2 fusion.16
  80.2 0.1 multiply_add_fusion.3
  80.3 0.1 reshape.113
  80.4 0.8 multiply_reduce_fusion.5
  81.3 36.5 %psum.43 = f32[8,16]{1,0:T(8,128)S(1)} all-reduce(f32[8,16]{1,0:T(8,128)S(1)} %broadcast_multiply_fusion.3), channel_id=1, replica_groups=mesh['tp'=16,'dp'=2] {'tp'}, use_global_device_ids=true, to_apply=%region_11.12 | all-reduce | flops 128 | bytes 1024 | tf_op jit(solution)/shard_map/psum | solution.py:100
  117.8 0.1 multiply_reduce_fusion.9
  117.9 0.8 multiply_convert_fusion.1
  118.7 1.8 all_gather.13
  120.5 2.6 fusion.9
  123.3 103.3 %all-reduce.11.cloned.1.call-done = f32[16,2048]{1,0:T(8,128)} async-done(((f32[16,2048]{1,0:T(8,128)}), f32[16,2048]{1,0:T(8,128)}) %all-reduce.11.cloned.1.call-update) | async-done | bytes 131088 | tf_op jit(solution)/shard_map/psum | solution.py:113
  226.6 1.0 fusion.62
  227.6 2.5 psum.45
  230.1 0.2 convolution_convert_fusion.1
  230.3 0.2 convolution_convert_fusion
  230.6 1.3 convolution_convert_fusion.2
  231.9 2.6 fusion.34
  234.5 2.6 fusion.37
  237.1 3.3 all-reduce.6
  240.5 0.6 stack.25
  241.2 4.7 %all-to-all-start.1 = ((bf16[16,8,128]{2,1,0:T(8,128)(2,1)}), bf16[16,8,128]{2,1,0:T(8,128)(2,1)S(1)}, u32[]{:S(2)}, u32[]{:S(2)}) async-start(bf16[16,8,128]{2,1,0:T(8,128)(2,1)} %stack.25), calls=%async_computation.4 | async-start | bytes 65536 | tf_op jit(solution)/shard_map/all_to_all | solution.py:70
  245.9 0.6 pad_maximum_fusion.4
  246.5 0.6 pad_maximum_fusion.5
  247.1 41.1 %all_gather.14 = bf16[8,2048]{1,0:T(8,128)(2,1)S(1)} all-gather(bf16[8,128]{1,0:T(8,128)(2,1)S(1)} %multiply_convert_fusion.3), channel_id=1, replica_groups=mesh['tp'=16,'dp'=2] {'tp'}, dimensions={1}, use_global_device_ids=true | all-gather | bytes 34816 | tf_op jit(solution)/shard_map/all_gather | solution.py:68
  288.2 0.2 reshape.114
  288.4 0.2 convert_reduce_fusion
  288.7 0.1 multiply_exponential_fusion
  288.9 0.7 multiply_reduce_fusion
  289.7 0.1 broadcast_multiply_fusion
  289.7 3.7 multiply_add_fusion.1
  293.4 2.3 pad_maximum_fusion
  295.8 0.2 reshape_reshape.7
  296.0 0.3 dynamic-slice_reduce_fusion
  296.3 4.2 fusion.7
  300.5 0.1 multiply_add_fusion.2
  300.6 0.8 multiply_reduce_fusion.2
  301.5 36.5 %psum.46 = f32[8,16]{1,0:T(8,128)S(1)} all-reduce(f32[8,16]{1,0:T(8,128)S(1)} %broadcast_multiply_fusion.2), channel_id=1, replica_groups=mesh['tp'=16,'dp'=2] {'tp'}, use_global_device_ids=true, to_apply=%region_25.26 | all-reduce | flops 128 | bytes 1024 | tf_op jit(solution)/shard_map/psum | solution.py:100
  338.1 0.1 multiply_reduce_fusion.8
  338.2 0.8 multiply_convert_fusion
  339.0 1.8 all_gather.15
  340.8 2.6 fusion
  343.5 0.6 pad_maximum_fusion.1
  344.1 102.8 %all-reduce.13.cloned.1.call-done = f32[16,2048]{1,0:T(8,128)} async-done(((f32[16,2048]{1,0:T(8,128)}), f32[16,2048]{1,0:T(8,128)}) %all-reduce.13.cloned.1.call-update) | async-done | bytes 131088 | tf_op jit(solution)/shard_map/psum | solution.py:113
  446.9 1.6 fusion.65
  (89 shorter events, 1.0 us)
Async XLA Ops:
  7.2 7.4 %copy-start = (bf16[16,2048]{1,0:T(8,128)(2,1)S(1)}, bf16[16,2048]{1,0:T(8,128)(2,1)}, u32[]{:S(2)}) copy-start(bf16[16,2048]{1,0:T(8,128)(2,1)} %param.19) | copy-start | bytes 196612
  7.2 7.4 %copy-start.8 = (bf16[2,4,128]{2,1,0:T(4,128)(2,1)S(1)}, bf16[2,4,128]{2,1,0:T(4,128)(2,1)}, u32[]{:S(2)}) copy-start(bf16[2,4,128]{2,1,0:T(4,128)(2,1)} %param.28) | copy-start | bytes 6148
  7.2 7.4 %copy-start.4 = (bf16[2,8,3,128]{3,1,2,0:T(8,128)(2,1)S(1)}, bf16[2,8,3,128]{3,1,2,0:T(8,128)(2,1)}, u32[]{:S(2)}) copy-start(bf16[2,8,3,128]{3,1,2,0:T(8,128)(2,1)} %param.36) | copy-start | bytes 36868
  7.2 7.4 %copy-start.13 = (bf16[2,2048,128]{2,1,0:T(8,128)(2,1)S(1)}, bf16[2,2048,128]{2,1,0:T(8,128)(2,1)}, u32[]{:S(2)}) copy-start(bf16[2,2048,128]{2,1,0:T(8,128)(2,1)} %param.23) | copy-start | bytes 3145732
  7.2 7.7 %copy-start.14 = (bf16[2,2048,128]{2,1,0:T(8,128)(2,1)S(1)}, bf16[2,2048,128]{2,1,0:T(8,128)(2,1)}, u32[]{:S(2)}) copy-start(bf16[2,2048,128]{2,1,0:T(8,128)(2,1)} %param.24) | copy-start | bytes 3145732
  7.2 67.4 %reduce-scatter.5.cloned.1.call-start = ((), (), s32[]{:S(2)}) async-start(), calls=%async_computation.6 | async-start | bytes 24576 | tf_op jit(solution)/shard_map/reduce_scatter | solution.py:48
  11.8 4.6 %copy-start.15 = (u32[32]{0:T(128)S(1)}, u32[32]{0:T(128)}, u32[]{:S(2)}) copy-start(u32[32]{0:T(128)} %constant.63) | copy-start | bytes 388
  14.6 18.1 %copy-start.10 = (f32[2,8]{1,0:T(2,128)S(1)}, f32[2,8]{1,0:T(2,128)}, u32[]{:S(2)}) copy-start(f32[2,8]{1,0:T(2,128)} %param.31) | copy-start | bytes 196
  14.6 18.1 %copy-start.9 = (bf16[2,4,128]{2,1,0:T(4,128)(2,1)S(1)}, bf16[2,4,128]{2,1,0:T(4,128)(2,1)}, u32[]{:S(2)}) copy-start(bf16[2,4,128]{2,1,0:T(4,128)(2,1)} %param.27) | copy-start | bytes 6148
  14.6 18.1 %copy-start.7 = (f32[2,512]{1,0:T(2,128)S(1)}, f32[2,512]{1,0:T(2,128)}, u32[]{:S(2)}) copy-start(f32[2,512]{1,0:T(2,128)} %param.32) | copy-start | bytes 12292
  14.6 18.1 %copy-start.5 = (bf16[2,8,3,128]{3,1,2,0:T(8,128)(2,1)S(1)}, bf16[2,8,3,128]{3,1,2,0:T(8,128)(2,1)}, u32[]{:S(2)}) copy-start(bf16[2,8,3,128]{3,1,2,0:T(8,128)(2,1)} %param.35) | copy-start | bytes 36868
  14.6 18.1 %copy-start.6 = (bf16[2,4,512]{2,1,0:T(4,128)(2,1)S(1)}, bf16[2,4,512]{2,1,0:T(4,128)(2,1)}, u32[]{:S(2)}) copy-start(bf16[2,4,512]{2,1,0:T(4,128)(2,1)} %param.26) | copy-start | bytes 24580
  14.9 59.0 %copy-start.1 = (bf16[2,8,3,512]{3,1,2,0:T(8,128)(2,1)S(1)}, bf16[2,8,3,512]{3,1,2,0:T(8,128)(2,1)}, u32[]{:S(2)}) copy-start(bf16[2,8,3,512]{3,1,2,0:T(8,128)(2,1)} %param.34) | copy-start | bytes 147460
  14.9 59.3 %copy-start.11 = (f32[2,8]{1,0:T(2,128)S(1)}, f32[2,8]{1,0:T(2,128)}, u32[]{:S(2)}) copy-start(f32[2,8]{1,0:T(2,128)} %param.30) | copy-start | bytes 196
  14.9 59.3 %copy-start.12 = (f32[2,8]{1,0:T(2,128)S(1)}, f32[2,8]{1,0:T(2,128)}, u32[]{:S(2)}) copy-start(f32[2,8]{1,0:T(2,128)} %param.29) | copy-start | bytes 196
  21.8 53.6 %all-to-all-start = ((bf16[16,8,128]{2,1,0:T(8,128)(2,1)}), bf16[16,8,128]{2,1,0:T(8,128)(2,1)S(1)}, u32[]{:S(2)}, u32[]{:S(2)}) async-start(bf16[16,8,128]{2,1,0:T(8,128)(2,1)} %stack.24), calls=%async_computation.1 | async-start | bytes 65536 | tf_op jit(solution)/shard_map/all_to_all | solution.py:70
  29.9 50.5 %reduce-scatter.7.cloned.1.call-start = ((), (), s32[]{:S(2)}) async-start(), calls=%async_computation.7 | async-start | bytes 24576 | tf_op jit(solution)/shard_map/reduce_scatter | solution.py:45
  32.6 194.0 %all-reduce.11.cloned.1.call-start = ((), (), s32[]{:S(2)}) async-start(), calls=%async_computation.8 | async-start | bytes 262144 | tf_op jit(solution)/shard_map/psum | solution.py:113
  76.0 47.3 %copy-start.2 = (bf16[8,512]{1,0:T(8,128)(2,1)S(1)}, bf16[8,512]{1,0:T(8,128)(2,1)}, u32[]{:S(2)}) copy-start(bf16[8,512]{1,0:T(8,128)(2,1)} %reduce-scatter.5.cloned.1.call-done) | copy-start | bytes 24580
  123.2 165.7 %reduce-scatter.9.cloned.1.call-start = ((), (), s32[]{:S(2)}) async-start(), calls=%async_computation.9 | async-start | bytes 24576 | tf_op jit(solution)/shard_map/reduce_scatter | solution.py:48
  241.2 54.6 %all-to-all-start.1 = ((bf16[16,8,128]{2,1,0:T(8,128)(2,1)}), bf16[16,8,128]{2,1,0:T(8,128)(2,1)S(1)}, u32[]{:S(2)}, u32[]{:S(2)}) async-start(bf16[16,8,128]{2,1,0:T(8,128)(2,1)} %stack.25), calls=%async_computation.4 | async-start | bytes 65536 | tf_op jit(solution)/shard_map/all_to_all | solution.py:70
  245.8 54.8 %reduce-scatter.11.cloned.1.call-start = ((), (), s32[]{:S(2)}) async-start(), calls=%async_computation.10 | async-start | bytes 24576 | tf_op jit(solution)/shard_map/reduce_scatter | solution.py:45
  288.7 158.2 %all-reduce.13.cloned.1.call-start = ((), (), s32[]{:S(2)}) async-start(), calls=%async_computation.11 | async-start | bytes 262144 | tf_op jit(solution)/shard_map/psum | solution.py:113
  296.2 47.2 %copy-start.3 = (bf16[8,512]{1,0:T(8,128)(2,1)S(1)}, bf16[8,512]{1,0:T(8,128)(2,1)}, u32[]{:S(2)}) copy-start(bf16[8,512]{1,0:T(8,128)(2,1)} %reduce-scatter.9.cloned.1.call-done) | copy-start | bytes 24580
Sparse Core Ops, SparseCore 0:
  14.7 10.0 reduce-scatter.4
  33.4 8.7 reduce-scatter.6
  123.3 103.2 all-reduce.10
  240.7 6.5 reduce-scatter.8
  288.8 3.3 reduce-scatter.10
  343.6 103.2 all-reduce.12
